TPU v7x, 32 devices: a whole 2x2x4 slice. The times are simulated.
32 devices in a mesh: sp: 8 (over z, x), tp: 4 (over y, core).
Axes of the slice: x: 2, y: 2, z: 4, core: 2. Of those that a mesh axis runs over, the one named last changes fastest.
Arguments:
- outer_gate: bfloat16 [512, 3072], P('tp', 'sp'), may hold values from -6 to 6
- inner_gate: bfloat16 [512, 3072], P('tp', 'sp'), may hold values from -6 to 6
- conv_input: bfloat16 [512, 3072], P('tp', 'sp'), may hold values from -6 to 6
- conv_taps: bfloat16 [3, 512], P(None, 'tp'), may hold values from -3.5 to 3.5
- mix_weight: bfloat16 [512, 2048], P(None, 'tp'), may hold values from -0.25 to 0.25
- residual: bfloat16 [3072, 2048], P('sp', 'tp'), may hold values from -24 to 24
- norm_gain: bfloat16 [2048], P('tp'), may hold values from 0.099609375 to 1.8984375
- routes: int32 [3072, 2], P('sp'), may hold values from 0 to 15, all different within a row; in each aligned block of 384 rows (0 to 383, 384 to 767, ...) at most 96 rows name the same one
- route_scores: float32 [3072, 2], P('sp'), may hold values from 0.05 to 1
- expert_gate: bfloat16 [16, 2048, 2048], P('sp', None, 'tp'), may hold values from -0.125 to 0.125
- expert_up: bfloat16 [16, 2048, 2048], P('sp', None, 'tp'), may hold values from -0.125 to 0.125
- expert_down: bfloat16 [16, 2048, 2048], P('sp', None, 'tp'), may hold values from -0.125 to 0.125
- shared_gate: bfloat16 [2048, 512], P(None, 'tp'), may hold values from -0.125 to 0.125
- shared_up: bfloat16 [2048, 512], P(None, 'tp'), may hold values from -0.125 to 0.125
- shared_down: bfloat16 [512, 2048], P(None, 'tp'), may hold values from -0.25 to 0.25
Outputs:
- layer_out: bfloat16 [3072, 2048], P('sp', 'tp')
Inputs may be any that keep to these rules, and one draw needn't show every extreme that they name: `routes`: within the rows of one index of sp (384 tokens), no expert is named by more than 96 of the token and choice pairs, a bound that some block reaches; the experts of one token differ.
All inputs are finite; a program needn't handle non-finite values.
Results may differ from a plain program's by a relative error of at most 0.014.
Values may be sent and summed in bfloat16 or wider, within the bound.
A program may use at most 64 MiB of HBM per device.

v0:
```python
import functools

import jax
import jax.numpy as jnp
from jax import lax
from jax.experimental import pallas as pl
from jax.experimental.pallas import tpu as pltpu
from jax.sharding import PartitionSpec as P

D = 2048


epsilon = 1e-06
routed_scale = 2.5


MESH = pl.DeviceIdType.MESH
VMEM_LIMIT = 58 * 2**20


def moe_kernel(
    n_sp,
    n_tp,
    outer,
    inner,
    conv,
    taps,
    mix,
    residual,
    gain,
    routes_rows,
    scores,
    gate_hbm,
    up_hbm,
    down_hbm,
    sgate,
    sup,
    sdown,
    out,
    ret,
    shared_out,
    outgoing,
    normed,
    stream,
    product,
    before,
    after,
    mixed,
    sums,
    recv,
    hid,
    whole,
    sact,
    obuf,
    gate_w,
    up_w,
    down_w,
    load_sem,
    own_sem,
    h_send,
    h_recv,
    a_send,
    a_recv,
    y_send,
    y_recv,
    d_send,
    d_recv,
    f_send,
    f_recv,
    r_send,
    r_recv,
):
    s = lax.axis_index("sp")
    t = lax.axis_index("tp")
    rows_y = n_tp // 2
    y, c = t // 2, lax.rem(t, 2)
    partner = y * 2 + (1 - c)
    experts, cap, width = outgoing.shape[1:]
    hidden_width = gate_w.shape[2]
    shared_width = sgate.shape[1]
    DISPATCH, HIDDEN = 0, n_sp
    WHOLE, SHARED, MIXED, SUMS = 2 * n_sp, 2 * n_sp + 1, 2 * n_sp + 2, 2 * n_sp + 3
    channels, tokens_here = outer.shape
    expert_count = n_sp * experts
    f32 = jnp.float32

    def y_peer(j):
        return lax.rem(y + j, rows_y) * 2

    def y_source(j):
        return lax.rem(y - j + rows_y, rows_y) * 2

    barrier = pltpu.get_barrier_semaphore()
    for j in range(1, n_sp):
        pl.semaphore_signal(barrier, inc=1, device_id=(lax.rem(s + j, n_sp), t), device_id_type=MESH)
    for j in range(1, rows_y):
        pl.semaphore_signal(barrier, inc=1, device_id=(s, y_peer(j) + c), device_id_type=MESH)
    pl.semaphore_signal(barrier, inc=1, device_id=(s, partner), device_id_type=MESH)

    filtered_input = inner[...].astype(f32) * conv[...].astype(f32)
    product[...] = filtered_input.astype(jnp.bfloat16)
    loads = [
        pltpu.make_async_copy(source, target, load_sem.at[i])
        for i, (source, target) in enumerate(((gate_hbm, gate_w), (up_hbm, up_w), (down_hbm, down_w)))
    ]
    for load in loads:
        load.start()
    pl.semaphore_wait(barrier, n_sp - 1 + rows_y - 1 + 1)

    def rows_of(k):
        return pl.ds(pl.multiple_of(lax.rem(s - k + n_sp, n_sp) * cap, cap), cap)

    def block(k, owner):
        return recv.at[:, rows_of(k), pl.ds(pl.multiple_of(owner * width, width), width)]

    def hidden_block(k, owner):
        return hid.at[:, rows_of(k), pl.ds(pl.multiple_of(owner * hidden_width, hidden_width), hidden_width)]

    def whole_block(k, owner):
        return whole.at[:, pl.ds(pl.multiple_of(owner * width, width), width)]

    def shared_block(k, owner):
        return sact.at[owner]

    def remote(source, target, send, receive, device):
        return pltpu.make_async_remote_copy(
            src_ref=source,
            dst_ref=target,
            send_sem=send,
            recv_sem=receive,
            device_id=device,
            device_id_type=MESH,
        )

    def y_copy(view, k, slot, j):
        return remote(view(k, t), view(k, t), y_send.at[slot], y_recv.at[slot], (s, y_peer(j) + c))

    def d_copy(view, k, slot):
        return remote(view(k, t), view(k, t), d_send.at[slot], d_recv.at[slot], (s, partner))

    def f_copy(view, k, slot, j):
        ref = view(k, y_source(j) + c)
        return remote(ref, ref, f_send.at[slot], f_recv.at[slot], (s, partner))

    def spread(view, k, slot):
        for j in range(1, rows_y):
            y_copy(view, k, slot, j).start()
        d_copy(view, k, slot).start()

    def forward(view, k, slot):
        for j in range(1, rows_y):
            y_copy(view, k, slot, j).wait_recv()
        for j in range(1, rows_y):
            f_copy(view, k, slot, j).start()

    def collect(view, k, slot):
        d_copy(view, k, slot).wait_recv()
        for j in range(1, rows_y):
            f_copy(view, k, slot, j).wait_recv()

    def finish_sends(view, k, slot):
        for j in range(1, rows_y):
            y_copy(view, k, slot, j).wait_send()
            f_copy(view, k, slot, j).wait_send()
        d_copy(view, k, slot).wait_send()

    def a_copy(k):
        peer = lax.rem(s + k, n_sp)
        rows = pl.ds(pl.multiple_of(s * cap, cap), cap)
        columns = pl.ds(pl.multiple_of(t * width, width), width)
        return remote(
            outgoing.at[peer], recv.at[:, rows, columns], a_send.at[k], a_recv.at[k], (peer, t)
        )

    def r_copy(k):
        peer = lax.rem(s - k + n_sp, n_sp)
        return remote(obuf.at[k], ret.at[s], r_send.at[k], r_recv.at[k], (peer, t))

    def column_of(row):
        return jnp.broadcast_to(row, (128, row.shape[1])).T[:, 0:1]

    def mixed_block(k, owner):
        return mixed.at[pl.ds(pl.multiple_of(owner * channels, channels), channels), :]

    def sums_block(k, owner):
        return sums.at[owner]

    edge = before.shape[1]
    up_copy = remote(
        product.at[:, pl.ds(tokens_here - edge, edge)], before, h_send.at[0], h_recv.at[0],
        (lax.rem(s + 1, n_sp), t),
    )
    down_copy = remote(
        product.at[:, pl.ds(0, edge)], after, h_send.at[1], h_recv.at[1],
        (lax.rem(s + n_sp - 1, n_sp), t),
    )
    up_copy.start()
    down_copy.start()

    token_i = lax.broadcasted_iota(jnp.int32, (tokens_here, tokens_here), 0)
    token_j = lax.broadcasted_iota(jnp.int32, (tokens_here, tokens_here), 1)
    choices = routes_rows.shape[0]
    one_row = [
        (routes_rows[k : k + 1, :] == lax.broadcasted_iota(jnp.int32, (expert_count, tokens_here), 0)).astype(f32)
        for k in range(choices)
    ]
    earlier_row = jnp.dot(
        sum(one_row).astype(jnp.bfloat16), (token_i < token_j).astype(f32).astype(jnp.bfloat16),
        preferred_element_type=f32,
    )
    slot_row = [
        routes_rows[k : k + 1, :] * cap + jnp.sum(earlier_row * one_row[k], axis=0, keepdims=True).astype(jnp.int32)
        for k in range(choices)
    ]
    slot_column = [column_of(slot_row[k].astype(f32)).astype(jnp.int32) for k in range(choices)]

    up_copy.wait_recv()
    down_copy.wait_recv()
    values = product[...].astype(f32)
    place = lax.broadcasted_iota(jnp.int32, (channels, tokens_here), 1)
    first = jnp.where(s == 0, 0.0, before[...].astype(f32)[:, edge - 1 : edge])
    last = jnp.where(s == n_sp - 1, 0.0, after[...].astype(f32)[:, 0:1])
    previous = jnp.where(place == 0, first, pltpu.roll(values, 1, 1))
    following = jnp.where(place == tokens_here - 1, last, pltpu.roll(values, tokens_here - 1, 1))
    tap = taps[...].astype(f32)
    filtered = (
        column_of(tap[0:1]) * previous + column_of(tap[1:2]) * values + column_of(tap[2:3]) * following
    )
    mixed[pl.ds(pl.multiple_of(t * channels, channels), channels), :] = (
        outer[...].astype(f32) * filtered
    ).astype(jnp.bfloat16)
    spread(mixed_block, 0, MIXED)
    forward(mixed_block, 0, MIXED)
    collect(mixed_block, 0, MIXED)
    projected = lax.dot_general(
        mixed[...], mix[...], (((0,), (0,)), ((), ())), preferred_element_type=f32
    )
    stream[...] = (residual[...].astype(f32) + projected).astype(jnp.bfloat16)
    levels = stream[...].astype(f32)
    own = jnp.broadcast_to(jnp.sum(levels * levels, axis=1, keepdims=True), (tokens_here, 128))
    sums[t] = own.T[:8]
    spread(sums_block, 0, SUMS)
    forward(sums_block, 0, SUMS)
    collect(sums_block, 0, SUMS)
    squares = sums[0]
    for j in range(1, n_tp):
        squares = squares + sums[j]
    squares = jnp.broadcast_to(squares[0:1], (128, tokens_here)).T[:, 0:1]
    inverse_rms = lax.rsqrt(squares / D + epsilon)
    normed[...] = (levels * inverse_rms * gain[...].astype(f32)).astype(jnp.bfloat16)

    def pack(peer):
        spot = lax.broadcasted_iota(jnp.int32, (experts * cap, tokens_here), 0) + peer * (experts * cap)
        chosen = sum((spot == slot_row[k]).astype(f32) for k in range(choices)).astype(jnp.bfloat16)
        packed = jnp.dot(chosen, normed[...], preferred_element_type=f32).astype(jnp.bfloat16)
        for e in range(experts):
            outgoing[peer, e] = packed[e * cap : (e + 1) * cap]

    own_whole = pltpu.make_async_copy(normed, whole_block(0, t), own_sem.at[0])
    own_whole.start()
    own_whole.wait()
    spread(whole_block, 0, WHOLE)
    pack(s)
    own_rows = pltpu.make_async_copy(outgoing.at[s], block(0, t), own_sem.at[1])
    own_rows.start()

    @pl.loop(1, n_sp)
    def _(k):
        pack(lax.rem(s + k, n_sp))
        a_copy(k).start()

    own_rows.wait()
    spread(block, 0, DISPATCH)
    forward(whole_block, 0, WHOLE)
    collect(whole_block, 0, WHOLE)
    tokens = whole[...]
    shared_hidden = jax.nn.silu(jnp.dot(tokens, sgate[...], preferred_element_type=jnp.float32)) * jnp.dot(
        tokens, sup[...], preferred_element_type=jnp.float32
    )
    sact[t] = shared_hidden.astype(jnp.bfloat16)
    spread(shared_block, 0, SHARED)
    for load in loads:
        load.wait()

    @pl.loop(1, n_sp + 4)
    def _(i):
        @pl.when(i < n_sp)
        def _():
            a_copy(i).wait_recv()
            spread(block, i, DISPATCH + i)

        @pl.when((i >= 1) & (i < n_sp + 1))
        def _():
            forward(block, i - 1, DISPATCH + i - 1)

        @pl.when((i >= 3) & (i < n_sp + 3))
        def _():
            forward(hidden_block, i - 3, HIDDEN + i - 3)

        @pl.when((i >= 2) & (i < n_sp + 2))
        def _():
            k = i - 2
            collect(block, k, DISPATCH + k)
            rows = rows_of(k)
            columns = pl.ds(pl.multiple_of(t * hidden_width, hidden_width), hidden_width)
            for e in range(experts):
                x = recv[e, rows, :]
                gate = jnp.dot(x, gate_w[e], preferred_element_type=jnp.float32)
                up = jnp.dot(x, up_w[e], preferred_element_type=jnp.float32)
                hid[e, rows, columns] = (jax.nn.silu(gate) * up).astype(jnp.bfloat16)
            spread(hidden_block, k, HIDDEN + k)

        @pl.when(i >= 4)
        def _():
            k = i - 4
            collect(hidden_block, k, HIDDEN + k)
            rows = rows_of(k)
            for e in range(experts):
                obuf[k, e] = jnp.dot(
                    hid[e, rows, :], down_w[e], preferred_element_type=jnp.float32
                ).astype(jnp.bfloat16)

            @pl.when(k > 0)
            def _():
                r_copy(k).start()

            @pl.when(k == 0)
            def _():
                ret[s] = obuf[0]

        @pl.when(i == 2)
        def _():
            forward(shared_block, 0, SHARED)

        @pl.when(i == 3)
        def _():
            collect(shared_block, 0, SHARED)
            total = jnp.zeros(shared_out.shape, jnp.float32)
            for j in range(n_tp):
                rows = sdown[pl.ds(j * shared_width, shared_width), :]
                total = total + jnp.dot(sact[j], rows, preferred_element_type=jnp.float32)
            shared_out[...] = total

    weight_rows = scores[...] / jnp.sum(scores[...], axis=0, keepdims=True) * routed_scale
    weights = [column_of(weight_rows[k : k + 1]) for k in range(choices)]

    @pl.loop(0, n_sp)
    def _(k):
        @pl.when(k > 0)
        def _():
            r_copy(k).wait_recv()

        group = lax.rem(s + k, n_sp)
        spot = lax.broadcasted_iota(jnp.int32, (tokens_here, experts * cap), 1) + group * (experts * cap)
        rows = ret[group].reshape(experts * cap, width)
        total = shared_out[...]
        for j in range(choices):
            chosen = (spot == slot_column[j]).astype(f32).astype(jnp.bfloat16)
            total = total + weights[j] * jnp.dot(chosen, rows, preferred_element_type=f32)
        shared_out[...] = total

    out[...] = (stream[...].astype(f32) + shared_out[...]).astype(jnp.bfloat16)

    up_copy.wait_send()
    down_copy.wait_send()
    finish_sends(mixed_block, 0, MIXED)
    finish_sends(sums_block, 0, SUMS)
    finish_sends(whole_block, 0, WHOLE)
    finish_sends(shared_block, 0, SHARED)

    @pl.loop(0, n_sp)
    def _(k):
        finish_sends(block, k, DISPATCH + k)
        finish_sends(hidden_block, k, HIDDEN + k)

        @pl.when(k > 0)
        def _():
            a_copy(k).wait_send()
            r_copy(k).wait_send()


def local(
    outer_gate,
    inner_gate,
    conv_input,
    conv_taps,
    mix_weight,
    residual,
    norm_gain,
    routes,
    route_scores,
    expert_gate,
    expert_up,
    expert_down,
    shared_gate,
    shared_up,
    shared_down,
):
    n_sp, n_tp = lax.axis_size("sp"), lax.axis_size("tp")
    experts, depth, hidden_width = expert_gate.shape
    channels, token_count = outer_gate.shape
    width = residual.shape[1]
    cap = 2 * token_count * routes.shape[1] // (experts * n_sp)
    cap = (cap + 15) // 16 * 16
    slots = 2 * n_sp + 4
    edge = min(128, token_count)
    vmem = pl.BlockSpec(memory_space=pltpu.VMEM)
    hbm = pl.BlockSpec(memory_space=pl.ANY)
    bf16 = jnp.bfloat16
    dma = pltpu.SemaphoreType.DMA
    return pl.pallas_call(
        functools.partial(moe_kernel, n_sp, n_tp),
        name="moe",
        out_shape=jax.ShapeDtypeStruct((token_count, width), bf16),
        in_specs=[vmem] * 9 + [hbm] * 3 + [vmem] * 3,
        out_specs=vmem,
        scratch_shapes=[
            pltpu.VMEM((n_sp, experts, cap, width), bf16),
            pltpu.VMEM((token_count, width), jnp.float32),
            pltpu.VMEM((n_sp, experts, cap, width), bf16),
            pltpu.VMEM((token_count, width), bf16),
            pltpu.VMEM((token_count, width), bf16),
            pltpu.VMEM((channels, token_count), bf16),
            pltpu.VMEM((channels, edge), bf16),
            pltpu.VMEM((channels, edge), bf16),
            pltpu.VMEM((channels * n_tp, token_count), bf16),
            pltpu.VMEM((n_tp, 8, token_count), jnp.float32),
            pltpu.VMEM((experts, n_sp * cap, width * n_tp), bf16),
            pltpu.VMEM((experts, n_sp * cap, hidden_width * n_tp), bf16),
            pltpu.VMEM((token_count, width * n_tp), bf16),
            pltpu.VMEM((n_tp, token_count, shared_gate.shape[1]), bf16),
            pltpu.VMEM((n_sp, experts, cap, width), bf16),
            pltpu.VMEM(expert_gate.shape, bf16),
            pltpu.VMEM(expert_up.shape, bf16),
            pltpu.VMEM(expert_down.shape, bf16),
            dma((3,)),
            dma((2,)),
            dma((2,)),
            dma((2,)),
            dma((n_sp,)),
            dma((n_sp,)),
            dma((slots,)),
            dma((slots,)),
            dma((slots,)),
            dma((slots,)),
            dma((slots,)),
            dma((slots,)),
            dma((n_sp,)),
            dma((n_sp,)),
        ],
        compiler_params=pltpu.CompilerParams(
            collective_id=0, has_side_effects=True, vmem_limit_bytes=VMEM_LIMIT
        ),
    )(
        outer_gate,
        inner_gate,
        conv_input,
        conv_taps,
        mix_weight,
        residual,
        norm_gain.reshape(1, width),
        routes.T,
        route_scores.T,
        expert_gate,
        expert_up,
        expert_down,
        shared_gate,
        shared_up,
        shared_down,
    )


def solution(mesh):
    in_specs = (
        P("tp", "sp"),
        P("tp", "sp"),
        P("tp", "sp"),
        P(None, "tp"),
        P(None, "tp"),
        P("sp", "tp"),
        P("tp"),
        P("sp", None),
        P("sp", None),
        P("sp", None, "tp"),
        P("sp", None, "tp"),
        P("sp", None, "tp"),
        P(None, "tp"),
        P(None, "tp"),
        P(None, "tp"),
    )
    out_specs = P("sp", "tp")
    return jax.shard_map(local, mesh=mesh, in_specs=in_specs, out_specs=out_specs, check_vma=False)
```

profile of v0, /device:TPU:0, one launch (start us, length us, event | category | flops | bytes accessed | tf_op | source)
XLA Modules:
  0.0 127.7 jit_solution(1932218691519611667)
XLA Ops:
  0.0 1.3 reshape.3.gain
  1.3 124.6 %moe.1 = bf16[384,512]{1,0:T(8,128)(2,1)} custom-call(bf16[128,384]{1,0:T(8,128)(2,1)} %outer.1, bf16[128,384]{1,0:T(8,128)(2,1)} %inner.1, bf16[128,384]{1,0:T(8,128)(2,1)} %conv.1, bf16[3,128]{1,0:T(4,128)(2,1)} %taps.1, bf16[512,512]{1,0:T(8,128)(2,1)} %mix.1, bf16[384,512]{1,0:T(8,128)(2,1)} %residual.1, bf16[1,512]{1,0:T(2,128)(2,1)} %reshape.3.gain, ...), custom_call_target="tpu_custom_call" | custom-call | tf_op jit(solution)/shard_map/moe/pallas_call | solution.py:411
  125.9 1.8 %copy.17 = bf16[384,512]{1,0:T(8,128)(2,1)} copy(bf16[384,512]{1,0:T(8,128)(2,1)} %moe.1) | data formatting | bytes 786432
where the time goes:
time: 128 us
  Pallas kernels  125 us (98%)
  local copies, waits for them, and re-layouts  3.03 us (2%)
    pallas_call x1, Pallas kernels, local(): pl.pallas_call(functools.partial(moe_kernel, n_sp, n_tp), name='moe', out...  125 us

commit v1 on v0

--- a/solution.py
+++ b/solution.py
@@ -40,6 +40,7 @@
     ret,
     shared_out,
     outgoing,
+    extra,
     normed,
     stream,
     product,
@@ -61,6 +62,8 @@
     h_recv,
     a_send,
     a_recv,
+    b_send,
+    b_recv,
     y_send,
     y_recv,
     d_send,
@@ -84,6 +87,22 @@
     expert_count = n_sp * experts
     f32 = jnp.float32
 
+    half = n_sp // 2
+    near = half if rows_y == 2 else 1
+    order = list(range(1, near)) + list(range(near, n_sp))
+    if near > 1:
+        order = [half, half + 1, 1, *range(half + 2, n_sp), *range(2, near)]
+
+    def chunk(i):
+        return sum(jnp.where(i == p + 1, k, 0) for p, k in enumerate(order))
+
+    def mate(k):
+        total, bit = 0, 1
+        while bit < n_sp:
+            total = total + lax.rem(s // bit + k // bit, 2) * bit
+            bit *= 2
+        return total
+
     def y_peer(j):
         return lax.rem(y + j, rows_y) * 2
 
@@ -92,7 +111,7 @@
 
     barrier = pltpu.get_barrier_semaphore()
     for j in range(1, n_sp):
-        pl.semaphore_signal(barrier, inc=1, device_id=(lax.rem(s + j, n_sp), t), device_id_type=MESH)
+        pl.semaphore_signal(barrier, inc=1, device_id=(mate(j), t), device_id_type=MESH)
     for j in range(1, rows_y):
         pl.semaphore_signal(barrier, inc=1, device_id=(s, y_peer(j) + c), device_id_type=MESH)
     pl.semaphore_signal(barrier, inc=1, device_id=(s, partner), device_id_type=MESH)
@@ -108,7 +127,7 @@
     pl.semaphore_wait(barrier, n_sp - 1 + rows_y - 1 + 1)
 
     def rows_of(k):
-        return pl.ds(pl.multiple_of(lax.rem(s - k + n_sp, n_sp) * cap, cap), cap)
+        return pl.ds(pl.multiple_of(mate(k) * cap, cap), cap)
 
     def block(k, owner):
         return recv.at[:, rows_of(k), pl.ds(pl.multiple_of(owner * width, width), width)]
@@ -165,16 +184,21 @@
         d_copy(view, k, slot).wait_send()
 
     def a_copy(k):
-        peer = lax.rem(s + k, n_sp)
         rows = pl.ds(pl.multiple_of(s * cap, cap), cap)
         columns = pl.ds(pl.multiple_of(t * width, width), width)
         return remote(
-            outgoing.at[peer], recv.at[:, rows, columns], a_send.at[k], a_recv.at[k], (peer, t)
+            outgoing.at[k], recv.at[:, rows, columns], a_send.at[k], a_recv.at[k], (mate(k), t)
         )
 
+    def b_copy(k, j):
+        rows = pl.ds(pl.multiple_of(s * cap, cap), cap)
+        columns = pl.ds(pl.multiple_of((y_source(j) + c) * width, width), width)
+        return remote(
+            extra.at[k, j - 1], recv.at[:, rows, columns], b_send.at[k, j], b_recv.at[k, j], (mate(k), t)
+        )
+
     def r_copy(k):
-        peer = lax.rem(s - k + n_sp, n_sp)
-        return remote(obuf.at[k], ret.at[s], r_send.at[k], r_recv.at[k], (peer, t))
+        return remote(obuf.at[k], ret.at[s], r_send.at[k], r_recv.at[k], (mate(k), t))
 
     def column_of(row):
         return jnp.broadcast_to(row, (128, row.shape[1])).T[:, 0:1]
@@ -249,70 +273,114 @@
     inverse_rms = lax.rsqrt(squares / D + epsilon)
     normed[...] = (levels * inverse_rms * gain[...].astype(f32)).astype(jnp.bfloat16)
 
-    def pack(peer):
+    def picked(peer):
         spot = lax.broadcasted_iota(jnp.int32, (experts * cap, tokens_here), 0) + peer * (experts * cap)
-        chosen = sum((spot == slot_row[k]).astype(f32) for k in range(choices)).astype(jnp.bfloat16)
-        packed = jnp.dot(chosen, normed[...], preferred_element_type=f32).astype(jnp.bfloat16)
-        for e in range(experts):
-            outgoing[peer, e] = packed[e * cap : (e + 1) * cap]
-
-    own_whole = pltpu.make_async_copy(normed, whole_block(0, t), own_sem.at[0])
+        return sum((spot == slot_row[k]).astype(f32) for k in range(choices)).astype(jnp.bfloat16)
+
+    def gathered(chosen, columns):
+        return jnp.dot(chosen, columns, preferred_element_type=f32).astype(jnp.bfloat16)
+
+    own_whole = pltpu.make_async_copy(normed, whole_block(0, t), own_sem)
     own_whole.start()
     own_whole.wait()
     spread(whole_block, 0, WHOLE)
-    pack(s)
-    own_rows = pltpu.make_async_copy(outgoing.at[s], block(0, t), own_sem.at[1])
-    own_rows.start()
 
     @pl.loop(1, n_sp)
-    def _(k):
-        pack(lax.rem(s + k, n_sp))
+    def _(q):
+        k = 1 + lax.rem(q - 2 + half, n_sp - 1)
+        packed = gathered(picked(mate(k)), normed[...])
+        for e in range(experts):
+            outgoing[k, e] = packed[e * cap : (e + 1) * cap]
         a_copy(k).start()
 
-    own_rows.wait()
-    spread(block, 0, DISPATCH)
     forward(whole_block, 0, WHOLE)
     collect(whole_block, 0, WHOLE)
+
+    def arrive(i):
+        k = chunk(i)
+        a_copy(k).wait_recv()
+
+        @pl.when(k >= near)
+        def _():
+            spread(block, k, DISPATCH + k)
+
+        @pl.when(k < near)
+        def _():
+            for j in range(1, rows_y):
+                b_copy(k, j).wait_recv()
+            d_copy(block, k, DISPATCH + k).start()
+            for j in range(1, rows_y):
+                f_copy(block, k, DISPATCH + k, j).start()
+
+    def pass_on(i):
+        k = chunk(i)
+
+        @pl.when(k >= near)
+        def _():
+            forward(block, k, DISPATCH + k)
+
+    def expert_in(k):
+        rows = rows_of(k)
+        columns = pl.ds(pl.multiple_of(t * hidden_width, hidden_width), hidden_width)
+        for e in range(experts):
+            x = recv[e, rows, :]
+            gate = jnp.dot(x, gate_w[e], preferred_element_type=jnp.float32)
+            up = jnp.dot(x, up_w[e], preferred_element_type=jnp.float32)
+            hid[e, rows, columns] = (jax.nn.silu(gate) * up).astype(jnp.bfloat16)
+        spread(hidden_block, k, HIDDEN + k)
+
+    arrive(1)
+
+    @pl.loop(1, near)
+    def _(k):
+        chosen = picked(mate(k))
+        for j in range(1, rows_y):
+            columns = pl.ds(pl.multiple_of((y_source(j) + c) * width, width), width)
+            packed = gathered(chosen, whole[:, columns])
+            for e in range(experts):
+                extra[k, j - 1, e] = packed[e * cap : (e + 1) * cap]
+            b_copy(k, j).start()
+
+    own_rows = gathered(picked(s), whole[...])
+    for e in range(experts):
+        recv[e, rows_of(0), :] = own_rows[e * cap : (e + 1) * cap]
+    for load in loads:
+        load.wait()
+    expert_in(0)
     tokens = whole[...]
     shared_hidden = jax.nn.silu(jnp.dot(tokens, sgate[...], preferred_element_type=jnp.float32)) * jnp.dot(
         tokens, sup[...], preferred_element_type=jnp.float32
     )
     sact[t] = shared_hidden.astype(jnp.bfloat16)
     spread(shared_block, 0, SHARED)
-    for load in loads:
-        load.wait()
-
-    @pl.loop(1, n_sp + 4)
+
+    weight_rows = scores[...] / jnp.sum(scores[...], axis=0, keepdims=True) * routed_scale
+    weights = [column_of(weight_rows[k : k + 1]) for k in range(choices)]
+
+    @pl.loop(2, n_sp + 6)
     def _(i):
+        @pl.when((i >= 3) & (i < n_sp + 2))
+        def _():
+            k = chunk(i - 2)
+            collect(block, k, DISPATCH + k)
+            expert_in(k)
+
         @pl.when(i < n_sp)
         def _():
-            a_copy(i).wait_recv()
-            spread(block, i, DISPATCH + i)
-
-        @pl.when((i >= 1) & (i < n_sp + 1))
-        def _():
-            forward(block, i - 1, DISPATCH + i - 1)
+            arrive(i)
+
+        @pl.when(i < n_sp + 1)
+        def _():
+            pass_on(i - 1)
 
         @pl.when((i >= 3) & (i < n_sp + 3))
         def _():
-            forward(hidden_block, i - 3, HIDDEN + i - 3)
-
-        @pl.when((i >= 2) & (i < n_sp + 2))
-        def _():
-            k = i - 2
-            collect(block, k, DISPATCH + k)
-            rows = rows_of(k)
-            columns = pl.ds(pl.multiple_of(t * hidden_width, hidden_width), hidden_width)
-            for e in range(experts):
-                x = recv[e, rows, :]
-                gate = jnp.dot(x, gate_w[e], preferred_element_type=jnp.float32)
-                up = jnp.dot(x, up_w[e], preferred_element_type=jnp.float32)
-                hid[e, rows, columns] = (jax.nn.silu(gate) * up).astype(jnp.bfloat16)
-            spread(hidden_block, k, HIDDEN + k)
-
-        @pl.when(i >= 4)
-        def _():
-            k = i - 4
+            k = chunk(i - 3)
+            forward(hidden_block, k, HIDDEN + k)
+
+        @pl.when((i >= 4) & (i < n_sp + 4))
+        def _():
+            k = chunk(i - 4)
             collect(hidden_block, k, HIDDEN + k)
             rows = rows_of(k)
             for e in range(experts):
@@ -328,11 +396,11 @@
             def _():
                 ret[s] = obuf[0]
 
-        @pl.when(i == 2)
+        @pl.when(i == 3)
         def _():
             forward(shared_block, 0, SHARED)
 
-        @pl.when(i == 3)
+        @pl.when(i == 4)
         def _():
             collect(shared_block, 0, SHARED)
             total = jnp.zeros(shared_out.shape, jnp.float32)
@@ -341,23 +409,22 @@
                 total = total + jnp.dot(sact[j], rows, preferred_element_type=jnp.float32)
             shared_out[...] = total
 
-    weight_rows = scores[...] / jnp.sum(scores[...], axis=0, keepdims=True) * routed_scale
-    weights = [column_of(weight_rows[k : k + 1]) for k in range(choices)]
-
-    @pl.loop(0, n_sp)
-    def _(k):
-        @pl.when(k > 0)
-        def _():
-            r_copy(k).wait_recv()
-
-        group = lax.rem(s + k, n_sp)
-        spot = lax.broadcasted_iota(jnp.int32, (tokens_here, experts * cap), 1) + group * (experts * cap)
-        rows = ret[group].reshape(experts * cap, width)
-        total = shared_out[...]
-        for j in range(choices):
-            chosen = (spot == slot_column[j]).astype(f32).astype(jnp.bfloat16)
-            total = total + weights[j] * jnp.dot(chosen, rows, preferred_element_type=f32)
-        shared_out[...] = total
+        @pl.when(i >= 6)
+        def _():
+            k = chunk(i - 6)
+
+            @pl.when(k > 0)
+            def _():
+                r_copy(k).wait_recv()
+
+            group = mate(k)
+            spot = lax.broadcasted_iota(jnp.int32, (tokens_here, experts * cap), 1) + group * (experts * cap)
+            rows = ret[group].reshape(experts * cap, width)
+            total = shared_out[...]
+            for j in range(choices):
+                chosen = (spot == slot_column[j]).astype(f32).astype(jnp.bfloat16)
+                total = total + weights[j] * jnp.dot(chosen, rows, preferred_element_type=f32)
+            shared_out[...] = total
 
     out[...] = (stream[...].astype(f32) + shared_out[...]).astype(jnp.bfloat16)
 
@@ -368,15 +435,24 @@
     finish_sends(whole_block, 0, WHOLE)
     finish_sends(shared_block, 0, SHARED)
 
-    @pl.loop(0, n_sp)
+    finish_sends(hidden_block, 0, HIDDEN)
+
+    @pl.loop(1, n_sp)
     def _(k):
-        finish_sends(block, k, DISPATCH + k)
         finish_sends(hidden_block, k, HIDDEN + k)
-
-        @pl.when(k > 0)
-        def _():
-            a_copy(k).wait_send()
-            r_copy(k).wait_send()
+        a_copy(k).wait_send()
+        r_copy(k).wait_send()
+
+        @pl.when(k >= near)
+        def _():
+            finish_sends(block, k, DISPATCH + k)
+
+        @pl.when(k < near)
+        def _():
+            d_copy(block, k, DISPATCH + k).wait_send()
+            for j in range(1, rows_y):
+                f_copy(block, k, DISPATCH + k, j).wait_send()
+                b_copy(k, j).wait_send()
 
 
 def local(
@@ -418,6 +494,7 @@
             pltpu.VMEM((n_sp, experts, cap, width), bf16),
             pltpu.VMEM((token_count, width), jnp.float32),
             pltpu.VMEM((n_sp, experts, cap, width), bf16),
+            pltpu.VMEM((n_sp // 2, n_tp // 2 - 1, experts, cap, width), bf16),
             pltpu.VMEM((token_count, width), bf16),
             pltpu.VMEM((token_count, width), bf16),
             pltpu.VMEM((channels, token_count), bf16),
@@ -434,11 +511,13 @@
             pltpu.VMEM(expert_up.shape, bf16),
             pltpu.VMEM(expert_down.shape, bf16),
             dma((3,)),
-            dma((2,)),
+            dma,
             dma((2,)),
             dma((2,)),
             dma((n_sp,)),
             dma((n_sp,)),
+            dma((n_sp // 2, n_tp // 2)),
+            dma((n_sp // 2, n_tp // 2)),
             dma((slots,)),
             dma((slots,)),
             dma((slots,)),

time: 128 us -> 118 us (0.922)
  Pallas kernels: 125 us -> 115 us
    pallas_call x1, Pallas kernels: 125 us -> 115 us  [local(): pl.pallas_call(functools.partial(moe_kernel, n_sp, n_tp), name='moe', out...]
where the time goes in v1:
time: 118 us
  Pallas kernels  115 us (97%)
  local copies, waits for them, and re-layouts  3.03 us (3%)
    pallas_call x1, Pallas kernels, local(): pl.pallas_call(functools.partial(moe_kernel, n_sp, n_tp), name='moe', out...  115 us

profile of v1, /device:TPU:0, one launch (start us, length us, event | category | flops | bytes accessed | tf_op | source)
XLA Modules:
  0.0 118.1 jit_solution(13054103139045654449)
XLA Ops:
  0.0 1.3 %reshape.3.gain = bf16[1,512]{1,0:T(2,128)(2,1)} reshape(bf16[512]{0:T(512)(128)(2,1)} %param.21) | data formatting | bytes 2048 | tf_op jit(solution)/shard_map/reshape | solution.py:540
  1.3 115.1 %moe.1 = bf16[384,512]{1,0:T(8,128)(2,1)} custom-call(bf16[128,384]{1,0:T(8,128)(2,1)} %outer.1, bf16[128,384]{1,0:T(8,128)(2,1)} %inner.1, bf16[128,384]{1,0:T(8,128)(2,1)} %conv.1, bf16[3,128]{1,0:T(4,128)(2,1)} %taps.1, bf16[512,512]{1,0:T(8,128)(2,1)} %mix.1, bf16[384,512]{1,0:T(8,128)(2,1)} %residual.1, bf16[1,512]{1,0:T(2,128)(2,1)} %reshape.3.gain, ...), custom_call_target="tpu_custom_call" | custom-call | tf_op jit(solution)/shard_map/moe/pallas_call | solution.py:487
  116.3 1.8 %copy.17 = bf16[384,512]{1,0:T(8,128)(2,1)} copy(bf16[384,512]{1,0:T(8,128)(2,1)} %moe.1) | data formatting | bytes 786432

commit v2 on v1

--- a/solution.py
+++ b/solution.py
@@ -21,21 +21,21 @@
 def moe_kernel(
     n_sp,
     n_tp,
-    outer,
-    inner,
-    conv,
-    taps,
-    mix,
-    residual,
-    gain,
-    routes_rows,
-    scores,
+    outer_hbm,
+    inner_hbm,
+    conv_hbm,
+    taps_hbm,
+    gain_hbm,
+    routes_hbm,
+    scores_hbm,
+    mix_hbm,
+    residual_hbm,
     gate_hbm,
     up_hbm,
     down_hbm,
-    sgate,
-    sup,
-    sdown,
+    sgate_hbm,
+    sup_hbm,
+    sdown_hbm,
     out,
     ret,
     shared_out,
@@ -48,14 +48,34 @@
     after,
     mixed,
     sums,
+    gains,
+    gain_row,
+    inverse_out,
+    inverse_in,
+    own_inverse,
+    far_inverse,
+    far_routes,
+    far_stream,
     recv,
     hid,
     whole,
     sact,
     obuf,
+    outer,
+    inner,
+    conv,
+    taps,
+    gain,
+    routes_rows,
+    scores,
+    mix,
+    residual,
     gate_w,
     up_w,
     down_w,
+    sgate,
+    sup,
+    sdown,
     load_sem,
     own_sem,
     h_send,
@@ -64,6 +84,10 @@
     a_recv,
     b_send,
     b_recv,
+    i_send,
+    i_recv,
+    p_send,
+    p_recv,
     y_send,
     y_recv,
     d_send,
@@ -82,19 +106,32 @@
     hidden_width = gate_w.shape[2]
     shared_width = sgate.shape[1]
     DISPATCH, HIDDEN = 0, n_sp
-    WHOLE, SHARED, MIXED, SUMS = 2 * n_sp, 2 * n_sp + 1, 2 * n_sp + 2, 2 * n_sp + 3
+    WHOLE, SHARED, MIXED, SUMS, GAINS = (2 * n_sp + j for j in range(5))
     channels, tokens_here = outer.shape
     expert_count = n_sp * experts
     f32 = jnp.float32
 
     half = n_sp // 2
-    near = half if rows_y == 2 else 1
-    order = list(range(1, near)) + list(range(near, n_sp))
-    if near > 1:
-        order = [half, half + 1, 1, *range(half + 2, n_sp), *range(2, near)]
+    near = half if rows_y == 2 else 2
+    quarter = half // 2
+    central = lax.rem((s // quarter + 1) // 2, 2)
+    order = [1, half, *range(2, half), *range(half + 1, n_sp)]
+    outer_order = order
+    combine = [0, *order]
+    if near > 2:
+        late = list(range(half + 2, n_sp))
+        order = [1, half, half + 1, *late, *range(2, near)]
+        outer_order = [1, half, *late, half + 1, *range(2, near)]
+        combine = [0, 1, half, late[0], half + 1, *late[1:], *range(2, near)]
+
+    def whole_rows(k):
+        return (k > 1) & (k < near)
+
+    def entry(table, i):
+        return sum(jnp.where(i == p, k, 0) for p, k in enumerate(table))
 
     def chunk(i):
-        return sum(jnp.where(i == p + 1, k, 0) for p, k in enumerate(order))
+        return central * entry([0, *order], i) + (1 - central) * entry([0, *outer_order], i)
 
     def mate(k):
         total, bit = 0, 1
@@ -116,14 +153,31 @@
         pl.semaphore_signal(barrier, inc=1, device_id=(s, y_peer(j) + c), device_id_type=MESH)
     pl.semaphore_signal(barrier, inc=1, device_id=(s, partner), device_id_type=MESH)
 
+    places = (
+        (inner_hbm, inner),
+        (conv_hbm, conv),
+        (gain_hbm, gain),
+        (routes_hbm, routes_rows),
+        (outer_hbm, outer),
+        (taps_hbm, taps),
+        (scores_hbm, scores),
+        (mix_hbm, mix),
+        (residual_hbm, residual),
+        (gate_hbm, gate_w),
+        (up_hbm, up_w),
+        (down_hbm, down_w),
+        (sgate_hbm, sgate),
+        (sup_hbm, sup),
+        (sdown_hbm, sdown),
+    )
+    loads = [pltpu.make_async_copy(source, target, load_sem.at[i]) for i, (source, target) in enumerate(places)]
+    for load in loads:
+        load.start()
+    for load in loads[:4]:
+        load.wait()
     filtered_input = inner[...].astype(f32) * conv[...].astype(f32)
     product[...] = filtered_input.astype(jnp.bfloat16)
-    loads = [
-        pltpu.make_async_copy(source, target, load_sem.at[i])
-        for i, (source, target) in enumerate(((gate_hbm, gate_w), (up_hbm, up_w), (down_hbm, down_w)))
-    ]
-    for load in loads:
-        load.start()
+    gains[t] = jnp.broadcast_to(gain[...].astype(f32).reshape(1, width), gains.shape[1:])
     pl.semaphore_wait(barrier, n_sp - 1 + rows_y - 1 + 1)
 
     def rows_of(k):
@@ -184,10 +238,12 @@
         d_copy(view, k, slot).wait_send()
 
     def a_copy(k):
-        rows = pl.ds(pl.multiple_of(s * cap, cap), cap)
         columns = pl.ds(pl.multiple_of(t * width, width), width)
+        relayed = k // half
+        source = mate(relayed * half)
+        rows = pl.ds(pl.multiple_of(source * cap, cap), cap)
         return remote(
-            outgoing.at[k], recv.at[:, rows, columns], a_send.at[k], a_recv.at[k], (mate(k), t)
+            outgoing.at[k], recv.at[:, rows, columns], a_send.at[k], a_recv.at[k], (mate(k - relayed * half), t)
         )
 
     def b_copy(k, j):
@@ -197,6 +253,16 @@
             extra.at[k, j - 1], recv.at[:, rows, columns], b_send.at[k, j], b_recv.at[k, j], (mate(k), t)
         )
 
+    def i_copy(k):
+        return remote(inverse_out.at[k], inverse_in.at[k], i_send.at[k], i_recv.at[k], (mate(k - k // half * half), t))
+
+    def p_copy(i, source, target):
+        return remote(source, target, p_send.at[i], p_recv.at[i], (mate(half), t))
+
+    routes_copy = p_copy(0, routes_rows, far_routes)
+    stream_copy = p_copy(1, stream, far_stream)
+    inverse_copy = p_copy(2, own_inverse, far_inverse)
+
     def r_copy(k):
         return remote(obuf.at[k], ret.at[s], r_send.at[k], r_recv.at[k], (mate(k), t))
 
@@ -208,6 +274,9 @@
 
     def sums_block(k, owner):
         return sums.at[owner]
+
+    def gains_block(k, owner):
+        return gains.at[owner]
 
     edge = before.shape[1]
     up_copy = remote(
@@ -220,24 +289,32 @@
     )
     up_copy.start()
     down_copy.start()
+    spread(gains_block, 0, GAINS)
+    routes_copy.start()
 
     token_i = lax.broadcasted_iota(jnp.int32, (tokens_here, tokens_here), 0)
     token_j = lax.broadcasted_iota(jnp.int32, (tokens_here, tokens_here), 1)
     choices = routes_rows.shape[0]
-    one_row = [
-        (routes_rows[k : k + 1, :] == lax.broadcasted_iota(jnp.int32, (expert_count, tokens_here), 0)).astype(f32)
-        for k in range(choices)
-    ]
-    earlier_row = jnp.dot(
-        sum(one_row).astype(jnp.bfloat16), (token_i < token_j).astype(f32).astype(jnp.bfloat16),
-        preferred_element_type=f32,
-    )
-    slot_row = [
-        routes_rows[k : k + 1, :] * cap + jnp.sum(earlier_row * one_row[k], axis=0, keepdims=True).astype(jnp.int32)
-        for k in range(choices)
-    ]
-    slot_column = [column_of(slot_row[k].astype(f32)).astype(jnp.int32) for k in range(choices)]
-
+
+    def slots_of(routes):
+        one_row = [
+            (routes[k : k + 1, :] == lax.broadcasted_iota(jnp.int32, (expert_count, tokens_here), 0)).astype(f32)
+            for k in range(choices)
+        ]
+        earlier_row = jnp.dot(
+            sum(one_row).astype(jnp.bfloat16), (token_i < token_j).astype(f32).astype(jnp.bfloat16),
+            preferred_element_type=f32,
+        )
+        rows = [
+            routes[k : k + 1, :] * cap + jnp.sum(earlier_row * one_row[k], axis=0, keepdims=True).astype(jnp.int32)
+            for k in range(choices)
+        ]
+        return rows, [column_of(row.astype(f32)).astype(jnp.int32) for row in rows]
+
+    slot_row, slot_column = slots_of(routes_rows[...])
+
+    for load in loads[4:7]:
+        load.wait()
     up_copy.wait_recv()
     down_copy.wait_recv()
     values = product[...].astype(f32)
@@ -256,6 +333,8 @@
     spread(mixed_block, 0, MIXED)
     forward(mixed_block, 0, MIXED)
     collect(mixed_block, 0, MIXED)
+    for load in loads[7:9]:
+        load.wait()
     projected = lax.dot_general(
         mixed[...], mix[...], (((0,), (0,)), ((), ())), preferred_element_type=f32
     )
@@ -264,47 +343,66 @@
     own = jnp.broadcast_to(jnp.sum(levels * levels, axis=1, keepdims=True), (tokens_here, 128))
     sums[t] = own.T[:8]
     spread(sums_block, 0, SUMS)
+    def picked(peer, slots):
+        spot = lax.broadcasted_iota(jnp.int32, (experts * cap, tokens_here), 0) + peer * (experts * cap)
+        return sum((spot == slots[k]).astype(f32) for k in range(choices)).astype(jnp.bfloat16)
+
+    def gathered(chosen, columns):
+        return jnp.dot(chosen, columns, preferred_element_type=f32).astype(jnp.bfloat16)
+
+    def pack(k, peer, slots, values):
+        packed = gathered(picked(peer, slots), values)
+        for e in range(experts):
+            outgoing[k, e] = packed[e * cap : (e + 1) * cap]
+        a_copy(k).start()
+
+    stream_copy.start()
+    own_whole = pltpu.make_async_copy(stream, whole_block(0, t), own_sem)
+    own_whole.start()
+    own_whole.wait()
+    spread(whole_block, 0, WHOLE)
+
+    @pl.loop(1, half)
+    def _(k):
+        pack(k, mate(k), slot_row, stream[...])
+
+    routes_copy.wait_recv()
+    far_row, far_column = slots_of(far_routes[...])
+    forward(gains_block, 0, GAINS)
     forward(sums_block, 0, SUMS)
+    collect(gains_block, 0, GAINS)
+    for j in range(n_tp):
+        gain_row[:, j * width : (j + 1) * width] = gains[j]
     collect(sums_block, 0, SUMS)
     squares = sums[0]
     for j in range(1, n_tp):
         squares = squares + sums[j]
-    squares = jnp.broadcast_to(squares[0:1], (128, tokens_here)).T[:, 0:1]
-    inverse_rms = lax.rsqrt(squares / D + epsilon)
-    normed[...] = (levels * inverse_rms * gain[...].astype(f32)).astype(jnp.bfloat16)
-
-    def picked(peer):
-        spot = lax.broadcasted_iota(jnp.int32, (experts * cap, tokens_here), 0) + peer * (experts * cap)
-        return sum((spot == slot_row[k]).astype(f32) for k in range(choices)).astype(jnp.bfloat16)
-
-    def gathered(chosen, columns):
-        return jnp.dot(chosen, columns, preferred_element_type=f32).astype(jnp.bfloat16)
-
-    own_whole = pltpu.make_async_copy(normed, whole_block(0, t), own_sem)
-    own_whole.start()
-    own_whole.wait()
-    spread(whole_block, 0, WHOLE)
-
-    @pl.loop(1, n_sp)
-    def _(q):
-        k = 1 + lax.rem(q - 2 + half, n_sp - 1)
-        packed = gathered(picked(mate(k)), normed[...])
-        for e in range(experts):
-            outgoing[k, e] = packed[e * cap : (e + 1) * cap]
-        a_copy(k).start()
-
-    forward(whole_block, 0, WHOLE)
-    collect(whole_block, 0, WHOLE)
+    inverse_row = lax.rsqrt(squares[0:1] / D + epsilon)
+    own_inverse[...] = jnp.broadcast_to(inverse_row, own_inverse.shape)
+    inverse_copy.start()
+    inverse_rms = column_of(inverse_row)
+
+    def inverses(peer, slots, values):
+        spot = lax.broadcasted_iota(jnp.int32, (tokens_here, inverse_in.shape[2]), 1) + peer * (experts * cap)
+        hits = sum(jnp.where(spot == slots[k], values, 0.0) for k in range(choices))
+        return jnp.broadcast_to(jnp.sum(hits, axis=0, keepdims=True), inverse_in.shape[1:])
+
+    inverse_in[0] = inverses(s, slot_column, inverse_rms)
+
+    @pl.loop(1, half)
+    def _(k):
+        inverse_out[k] = inverses(mate(k), slot_column, inverse_rms)
+        i_copy(k).start()
 
     def arrive(i):
         k = chunk(i)
         a_copy(k).wait_recv()
 
-        @pl.when(k >= near)
+        @pl.when(jnp.logical_not(whole_rows(k)))
         def _():
             spread(block, k, DISPATCH + k)
 
-        @pl.when(k < near)
+        @pl.when(whole_rows(k))
         def _():
             for j in range(1, rows_y):
                 b_copy(k, j).wait_recv()
@@ -315,25 +413,35 @@
     def pass_on(i):
         k = chunk(i)
 
-        @pl.when(k >= near)
+        @pl.when(jnp.logical_not(whole_rows(k)))
         def _():
             forward(block, k, DISPATCH + k)
+
+    arrive(1)
+    forward(whole_block, 0, WHOLE)
+    collect(whole_block, 0, WHOLE)
 
     def expert_in(k):
         rows = rows_of(k)
         columns = pl.ds(pl.multiple_of(t * hidden_width, hidden_width), hidden_width)
+        inverse = column_of(inverse_in[k][0:1])
         for e in range(experts):
-            x = recv[e, rows, :]
+            x = recv[e, rows, :].astype(f32) * inverse[e * cap : (e + 1) * cap] * gain_row[0:1]
+            x = x.astype(jnp.bfloat16)
             gate = jnp.dot(x, gate_w[e], preferred_element_type=jnp.float32)
             up = jnp.dot(x, up_w[e], preferred_element_type=jnp.float32)
             hid[e, rows, columns] = (jax.nn.silu(gate) * up).astype(jnp.bfloat16)
         spread(hidden_block, k, HIDDEN + k)
 
-    arrive(1)
-
-    @pl.loop(1, near)
-    def _(k):
-        chosen = picked(mate(k))
+    own_rows = gathered(picked(s, slot_row), whole[...])
+    for e in range(experts):
+        recv[e, rows_of(0), :] = own_rows[e * cap : (e + 1) * cap]
+    for load in loads[9:]:
+        load.wait()
+    expert_in(0)
+
+    def pack_extra(k):
+        chosen = picked(mate(k), slot_row)
         for j in range(1, rows_y):
             columns = pl.ds(pl.multiple_of((y_source(j) + c) * width, width), width)
             packed = gathered(chosen, whole[:, columns])
@@ -341,46 +449,66 @@
                 extra[k, j - 1, e] = packed[e * cap : (e + 1) * cap]
             b_copy(k, j).start()
 
-    own_rows = gathered(picked(s), whole[...])
+    def take(i):
+        k = chunk(i)
+        pass_on(i)
+
+        @pl.when(k != half)
+        def _():
+            i_copy(k).wait_recv()
+
+        collect(block, k, DISPATCH + k)
+        expert_in(k)
+
+    take(1)
+    stream_copy.wait_recv()
+
+    @pl.loop(half + 1, n_sp)
+    def _(k):
+        pack(k, mate(k - half), far_row, far_stream[...])
+
+    far_rows = gathered(picked(s, far_row), far_stream[...])
     for e in range(experts):
-        recv[e, rows_of(0), :] = own_rows[e * cap : (e + 1) * cap]
-    for load in loads:
-        load.wait()
-    expert_in(0)
-    tokens = whole[...]
+        recv[e, rows_of(half), pl.ds(pl.multiple_of(t * width, width), width)] = far_rows[e * cap : (e + 1) * cap]
+    spread(block, half, DISPATCH + half)
+    @pl.loop(2, near)
+    def _(k):
+        pack_extra(k)
+
+    normed[...] = (whole[...].astype(f32) * inverse_rms * gain_row[0:1]).astype(jnp.bfloat16)
+    tokens = normed[...]
     shared_hidden = jax.nn.silu(jnp.dot(tokens, sgate[...], preferred_element_type=jnp.float32)) * jnp.dot(
         tokens, sup[...], preferred_element_type=jnp.float32
     )
     sact[t] = shared_hidden.astype(jnp.bfloat16)
     spread(shared_block, 0, SHARED)
 
+    inverse_copy.wait_recv()
+    far_rms = column_of(far_inverse[0:1])
+    inverse_in[half] = inverses(s, far_column, far_rms)
+
+    @pl.loop(half + 1, n_sp)
+    def _(k):
+        inverse_out[k] = inverses(mate(k - half), far_column, far_rms)
+        i_copy(k).start()
+
     weight_rows = scores[...] / jnp.sum(scores[...], axis=0, keepdims=True) * routed_scale
     weights = [column_of(weight_rows[k : k + 1]) for k in range(choices)]
 
-    @pl.loop(2, n_sp + 6)
+    @pl.loop(2, n_sp + 7)
     def _(i):
-        @pl.when((i >= 3) & (i < n_sp + 2))
+        @pl.when((i > 2) & (i < n_sp))
+        def _():
+            arrive(i)
+
+        @pl.when((i > 2) & (i < n_sp + 1))
+        def _():
+            take(i - 1)
+
+        @pl.when(i < n_sp + 2)
         def _():
             k = chunk(i - 2)
-            collect(block, k, DISPATCH + k)
-            expert_in(k)
-
-        @pl.when(i < n_sp)
-        def _():
-            arrive(i)
-
-        @pl.when(i < n_sp + 1)
-        def _():
-            pass_on(i - 1)
-
-        @pl.when((i >= 3) & (i < n_sp + 3))
-        def _():
-            k = chunk(i - 3)
             forward(hidden_block, k, HIDDEN + k)
-
-        @pl.when((i >= 4) & (i < n_sp + 4))
-        def _():
-            k = chunk(i - 4)
             collect(hidden_block, k, HIDDEN + k)
             rows = rows_of(k)
             for e in range(experts):
@@ -409,9 +537,9 @@
                 total = total + jnp.dot(sact[j], rows, preferred_element_type=jnp.float32)
             shared_out[...] = total
 
-        @pl.when(i >= 6)
-        def _():
-            k = chunk(i - 6)
+        @pl.when(i >= 7)
+        def _():
+            k = entry(combine, i - 7)
 
             @pl.when(k > 0)
             def _():
@@ -428,10 +556,14 @@
 
     out[...] = (stream[...].astype(f32) + shared_out[...]).astype(jnp.bfloat16)
 
+    routes_copy.wait_send()
+    stream_copy.wait_send()
+    inverse_copy.wait_send()
     up_copy.wait_send()
     down_copy.wait_send()
     finish_sends(mixed_block, 0, MIXED)
     finish_sends(sums_block, 0, SUMS)
+    finish_sends(gains_block, 0, GAINS)
     finish_sends(whole_block, 0, WHOLE)
     finish_sends(shared_block, 0, SHARED)
 
@@ -440,14 +572,18 @@
     @pl.loop(1, n_sp)
     def _(k):
         finish_sends(hidden_block, k, HIDDEN + k)
-        a_copy(k).wait_send()
         r_copy(k).wait_send()
 
-        @pl.when(k >= near)
+        @pl.when(k != half)
+        def _():
+            a_copy(k).wait_send()
+            i_copy(k).wait_send()
+
+        @pl.when(jnp.logical_not(whole_rows(k)))
         def _():
             finish_sends(block, k, DISPATCH + k)
 
-        @pl.when(k < near)
+        @pl.when(whole_rows(k))
         def _():
             d_copy(block, k, DISPATCH + k).wait_send()
             for j in range(1, rows_y):
@@ -478,39 +614,60 @@
     width = residual.shape[1]
     cap = 2 * token_count * routes.shape[1] // (experts * n_sp)
     cap = (cap + 15) // 16 * 16
-    slots = 2 * n_sp + 4
+    slots = 2 * n_sp + 5
     edge = min(128, token_count)
+    lanes = (experts * cap + 127) // 128 * 128
     vmem = pl.BlockSpec(memory_space=pltpu.VMEM)
-    hbm = pl.BlockSpec(memory_space=pl.ANY)
+    hbm = pl.BlockSpec(memory_space=pltpu.HBM)
     bf16 = jnp.bfloat16
     dma = pltpu.SemaphoreType.DMA
     return pl.pallas_call(
         functools.partial(moe_kernel, n_sp, n_tp),
         name="moe",
-        out_shape=jax.ShapeDtypeStruct((token_count, width), bf16),
-        in_specs=[vmem] * 9 + [hbm] * 3 + [vmem] * 3,
+        out_shape=pltpu.VMEM((token_count, width), bf16),
+        in_specs=[hbm] * 15,
         out_specs=vmem,
         scratch_shapes=[
             pltpu.VMEM((n_sp, experts, cap, width), bf16),
             pltpu.VMEM((token_count, width), jnp.float32),
             pltpu.VMEM((n_sp, experts, cap, width), bf16),
             pltpu.VMEM((n_sp // 2, n_tp // 2 - 1, experts, cap, width), bf16),
-            pltpu.VMEM((token_count, width), bf16),
+            pltpu.VMEM((token_count, width * n_tp), bf16),
             pltpu.VMEM((token_count, width), bf16),
             pltpu.VMEM((channels, token_count), bf16),
             pltpu.VMEM((channels, edge), bf16),
             pltpu.VMEM((channels, edge), bf16),
             pltpu.VMEM((channels * n_tp, token_count), bf16),
             pltpu.VMEM((n_tp, 8, token_count), jnp.float32),
+            pltpu.VMEM((n_tp, 8, width), jnp.float32),
+            pltpu.VMEM((8, width * n_tp), jnp.float32),
+            pltpu.VMEM((n_sp, 8, lanes), jnp.float32),
+            pltpu.VMEM((n_sp, 8, lanes), jnp.float32),
+            pltpu.VMEM((8, token_count), jnp.float32),
+            pltpu.VMEM((8, token_count), jnp.float32),
+            pltpu.VMEM((routes.shape[1], token_count), jnp.int32),
+            pltpu.VMEM((token_count, width), bf16),
             pltpu.VMEM((experts, n_sp * cap, width * n_tp), bf16),
             pltpu.VMEM((experts, n_sp * cap, hidden_width * n_tp), bf16),
             pltpu.VMEM((token_count, width * n_tp), bf16),
             pltpu.VMEM((n_tp, token_count, shared_gate.shape[1]), bf16),
             pltpu.VMEM((n_sp, experts, cap, width), bf16),
+            pltpu.VMEM(outer_gate.shape, bf16),
+            pltpu.VMEM(inner_gate.shape, bf16),
+            pltpu.VMEM(conv_input.shape, bf16),
+            pltpu.VMEM(conv_taps.shape, bf16),
+            pltpu.VMEM(norm_gain.shape, bf16),
+            pltpu.VMEM(routes.shape[::-1], jnp.int32),
+            pltpu.VMEM(route_scores.shape[::-1], jnp.float32),
+            pltpu.VMEM(mix_weight.shape, bf16),
+            pltpu.VMEM(residual.shape, bf16),
             pltpu.VMEM(expert_gate.shape, bf16),
             pltpu.VMEM(expert_up.shape, bf16),
             pltpu.VMEM(expert_down.shape, bf16),
-            dma((3,)),
+            pltpu.VMEM(shared_gate.shape, bf16),
+            pltpu.VMEM(shared_up.shape, bf16),
+            pltpu.VMEM(shared_down.shape, bf16),
+            dma((15,)),
             dma,
             dma((2,)),
             dma((2,)),
@@ -518,6 +675,10 @@
             dma((n_sp,)),
             dma((n_sp // 2, n_tp // 2)),
             dma((n_sp // 2, n_tp // 2)),
+            dma((n_sp,)),
+            dma((n_sp,)),
+            dma((3,)),
+            dma((3,)),
             dma((slots,)),
             dma((slots,)),
             dma((slots,)),
@@ -535,11 +696,11 @@
         inner_gate,
         conv_input,
         conv_taps,
+        norm_gain,
+        routes.T,
+        route_scores.T,
         mix_weight,
         residual,
-        norm_gain.reshape(1, width),
-        routes.T,
-        route_scores.T,
         expert_gate,
         expert_up,
         expert_down,

time: 118 us -> 97.8 us (0.83)
  Pallas kernels: 115 us -> 96.9 us
  local copies, waits for them, and re-layouts: 3.03 us -> 0.75 us
    pallas_call x1, Pallas kernels: 115 us -> 96.9 us  [local(): pl.pallas_call(functools.partial(moe_kernel, n_sp, n_tp), name='moe', out...]
    reshape x1 -> x0, local copies, waits for them, and re-layouts: 1.26 us -> none  [local(): norm_gain.reshape(1, width)]
where the time goes in v2:
time: 97.8 us; the launch traced here: 97.7 us
  Pallas kernels  96.9 us (99%)
    pallas_call x1, Pallas kernels, local(): pl.pallas_call(functools.partial(moe_kernel, n_sp, n_tp), name='moe', out...  96.9 us

profile of v2, /device:TPU:0, one launch (start us, length us, event | category | flops | bytes accessed | tf_op | source)
XLA Modules:
  0.0 97.7 jit_solution(213498005652067836)
XLA Ops:
  0.0 96.9 %moe.1 = bf16[384,512]{1,0:T(8,128)(2,1)S(1)} custom-call(bf16[128,384]{1,0:T(8,128)(2,1)} %outer_hbm.1, bf16[128,384]{1,0:T(8,128)(2,1)} %inner_hbm.1, bf16[128,384]{1,0:T(8,128)(2,1)} %conv_hbm.1, bf16[3,128]{1,0:T(4,128)(2,1)} %taps_hbm.1, bf16[512]{0:T(512)(128)(2,1)} %gain_hbm.1, s32[2,384]{1,0:T(2,128)} %bitcast.2, f32[2,384]{1,0:T(2,128)} %bitcast.3, ...), custom_call_target="tpu_custom_call" | custom-call | tf_op jit(solution)/shard_map/moe/pallas_call | solution.py:624
  96.9 0.7 copy.17

commit v3 on v2

--- a/solution.py
+++ b/solution.py
@@ -47,6 +47,8 @@
     before,
     after,
     mixed,
+    edges,
+    patched,
     sums,
     gains,
     gain_row,
@@ -106,7 +108,7 @@
     hidden_width = gate_w.shape[2]
     shared_width = sgate.shape[1]
     DISPATCH, HIDDEN = 0, n_sp
-    WHOLE, SHARED, MIXED, SUMS, GAINS = (2 * n_sp + j for j in range(5))
+    WHOLE, SHARED, MIXED, SUMS, GAINS, EDGES = (n_sp * (1 + experts) + j for j in range(6))
     channels, tokens_here = outer.shape
     expert_count = n_sp * experts
     f32 = jnp.float32
@@ -120,9 +122,10 @@
     combine = [0, *order]
     if near > 2:
         late = list(range(half + 2, n_sp))
-        order = [1, half, half + 1, *late, *range(2, near)]
-        outer_order = [1, half, *late, half + 1, *range(2, near)]
-        combine = [0, 1, half, late[0], half + 1, *late[1:], *range(2, near)]
+        nearest = list(range(2, near))
+        order = [1, half, half + 1, *late, *nearest]
+        outer_order = [1, half, *late, half + 1, *nearest]
+        combine = [0, 1, half, late[0], half + 1, *late[1:], *nearest]
 
     def whole_rows(k):
         return (k > 1) & (k < near)
@@ -186,8 +189,12 @@
     def block(k, owner):
         return recv.at[:, rows_of(k), pl.ds(pl.multiple_of(owner * width, width), width)]
 
-    def hidden_block(k, owner):
-        return hid.at[:, rows_of(k), pl.ds(pl.multiple_of(owner * hidden_width, hidden_width), hidden_width)]
+    def hidden_block(e):
+        def view(k, owner):
+            columns = pl.ds(pl.multiple_of(owner * hidden_width, hidden_width), hidden_width)
+            return hid.at[e, rows_of(k), columns]
+
+        return view
 
     def whole_block(k, owner):
         return whole.at[:, pl.ds(pl.multiple_of(owner * width, width), width)]
@@ -263,14 +270,17 @@
     stream_copy = p_copy(1, stream, far_stream)
     inverse_copy = p_copy(2, own_inverse, far_inverse)
 
-    def r_copy(k):
-        return remote(obuf.at[k], ret.at[s], r_send.at[k], r_recv.at[k], (mate(k), t))
+    def r_copy(k, e):
+        return remote(obuf.at[k, e], ret.at[s, e], r_send.at[k, e], r_recv.at[k, e], (mate(k), t))
 
     def column_of(row):
         return jnp.broadcast_to(row, (128, row.shape[1])).T[:, 0:1]
 
     def mixed_block(k, owner):
         return mixed.at[pl.ds(pl.multiple_of(owner * channels, channels), channels), :]
+
+    def edges_block(k, owner):
+        return edges.at[owner]
 
     def sums_block(k, owner):
         return sums.at[owner]
@@ -291,6 +301,22 @@
     down_copy.start()
     spread(gains_block, 0, GAINS)
     routes_copy.start()
+
+    for load in loads[4:7]:
+        load.wait()
+    values = product[...].astype(f32)
+    place = lax.broadcasted_iota(jnp.int32, (channels, tokens_here), 1)
+    tap = taps[...].astype(f32)
+    tap_columns = [column_of(tap[j : j + 1]) for j in range(3)]
+
+    def gated(first, last):
+        previous = jnp.where(place == 0, first, pltpu.roll(values, 1, 1))
+        following = jnp.where(place == tokens_here - 1, last, pltpu.roll(values, tokens_here - 1, 1))
+        filtered = tap_columns[0] * previous + tap_columns[1] * values + tap_columns[2] * following
+        return (outer[...].astype(f32) * filtered).astype(jnp.bfloat16)
+
+    mixed[pl.ds(pl.multiple_of(t * channels, channels), channels), :] = gated(0.0, 0.0)
+    spread(mixed_block, 0, MIXED)
 
     token_i = lax.broadcasted_iota(jnp.int32, (tokens_here, tokens_here), 0)
     token_j = lax.broadcasted_iota(jnp.int32, (tokens_here, tokens_here), 1)
@@ -313,30 +339,30 @@
 
     slot_row, slot_column = slots_of(routes_rows[...])
 
-    for load in loads[4:7]:
-        load.wait()
     up_copy.wait_recv()
     down_copy.wait_recv()
-    values = product[...].astype(f32)
-    place = lax.broadcasted_iota(jnp.int32, (channels, tokens_here), 1)
     first = jnp.where(s == 0, 0.0, before[...].astype(f32)[:, edge - 1 : edge])
     last = jnp.where(s == n_sp - 1, 0.0, after[...].astype(f32)[:, 0:1])
-    previous = jnp.where(place == 0, first, pltpu.roll(values, 1, 1))
-    following = jnp.where(place == tokens_here - 1, last, pltpu.roll(values, tokens_here - 1, 1))
-    tap = taps[...].astype(f32)
-    filtered = (
-        column_of(tap[0:1]) * previous + column_of(tap[1:2]) * values + column_of(tap[2:3]) * following
-    )
-    mixed[pl.ds(pl.multiple_of(t * channels, channels), channels), :] = (
-        outer[...].astype(f32) * filtered
-    ).astype(jnp.bfloat16)
-    spread(mixed_block, 0, MIXED)
+    complete = gated(first, last).astype(f32)
+    left = lax.broadcasted_iota(jnp.int32, (channels, edge), 1) < edge // 2
+    edges[t] = jnp.where(left, complete[:, :edge], complete[:, tokens_here - edge :]).astype(jnp.bfloat16)
+    spread(edges_block, 0, EDGES)
     forward(mixed_block, 0, MIXED)
+    forward(edges_block, 0, EDGES)
     collect(mixed_block, 0, MIXED)
+    collect(edges_block, 0, EDGES)
+    patched[...] = mixed[...]
+    for j in range(n_tp):
+        rows = slice(j * channels, (j + 1) * channels)
+        border = edges[j].astype(f32)
+        start = patched[rows, :edge].astype(f32)
+        patched[rows, :edge] = jnp.where(left, border, start).astype(jnp.bfloat16)
+        end = patched[rows, tokens_here - edge :].astype(f32)
+        patched[rows, tokens_here - edge :] = jnp.where(left, end, border).astype(jnp.bfloat16)
     for load in loads[7:9]:
         load.wait()
     projected = lax.dot_general(
-        mixed[...], mix[...], (((0,), (0,)), ((), ())), preferred_element_type=f32
+        patched[...], mix[...], (((0,), (0,)), ((), ())), preferred_element_type=f32
     )
     stream[...] = (residual[...].astype(f32) + projected).astype(jnp.bfloat16)
     levels = stream[...].astype(f32)
@@ -431,7 +457,7 @@
             gate = jnp.dot(x, gate_w[e], preferred_element_type=jnp.float32)
             up = jnp.dot(x, up_w[e], preferred_element_type=jnp.float32)
             hid[e, rows, columns] = (jax.nn.silu(gate) * up).astype(jnp.bfloat16)
-        spread(hidden_block, k, HIDDEN + k)
+            spread(hidden_block(e), k, HIDDEN + k * experts + e)
 
     own_rows = gathered(picked(s, slot_row), whole[...])
     for e in range(experts):
@@ -495,30 +521,45 @@
     weight_rows = scores[...] / jnp.sum(scores[...], axis=0, keepdims=True) * routed_scale
     weights = [column_of(weight_rows[k : k + 1]) for k in range(choices)]
 
-    @pl.loop(2, n_sp + 7)
+    def returned(k):
+        group = mate(k)
+        spot = lax.broadcasted_iota(jnp.int32, (tokens_here, experts * cap), 1) + group * (experts * cap)
+        rows = ret[group].reshape(experts * cap, width)
+        total = shared_out[...]
+        for j in range(choices):
+            chosen = (spot == slot_column[j]).astype(f32).astype(jnp.bfloat16)
+            total = total + weights[j] * jnp.dot(chosen, rows, preferred_element_type=f32)
+        return total
+
+    @pl.loop(2, n_sp + 6)
     def _(i):
         @pl.when((i > 2) & (i < n_sp))
         def _():
             arrive(i)
 
-        @pl.when((i > 2) & (i < n_sp + 1))
-        def _():
-            take(i - 1)
+        early = jnp.where(i >= n_sp - 1, 1, 0)
+        ahead = jnp.where(i >= n_sp - 2, 1, 0)
+
+        @pl.when((i > 2) & (i < n_sp))
+        def _():
+            @pl.loop(i - 1 + early, i + ahead)
+            def _(p):
+                take(p)
 
         @pl.when(i < n_sp + 2)
         def _():
             k = chunk(i - 2)
-            forward(hidden_block, k, HIDDEN + k)
-            collect(hidden_block, k, HIDDEN + k)
             rows = rows_of(k)
             for e in range(experts):
+                forward(hidden_block(e), k, HIDDEN + k * experts + e)
+                collect(hidden_block(e), k, HIDDEN + k * experts + e)
                 obuf[k, e] = jnp.dot(
                     hid[e, rows, :], down_w[e], preferred_element_type=jnp.float32
                 ).astype(jnp.bfloat16)
 
-            @pl.when(k > 0)
-            def _():
-                r_copy(k).start()
+                @pl.when(k > 0)
+                def _():
+                    r_copy(k, e).start()
 
             @pl.when(k == 0)
             def _():
@@ -543,18 +584,10 @@
 
             @pl.when(k > 0)
             def _():
-                r_copy(k).wait_recv()
-
-            group = mate(k)
-            spot = lax.broadcasted_iota(jnp.int32, (tokens_here, experts * cap), 1) + group * (experts * cap)
-            rows = ret[group].reshape(experts * cap, width)
-            total = shared_out[...]
-            for j in range(choices):
-                chosen = (spot == slot_column[j]).astype(f32).astype(jnp.bfloat16)
-                total = total + weights[j] * jnp.dot(chosen, rows, preferred_element_type=f32)
-            shared_out[...] = total
-
-    out[...] = (stream[...].astype(f32) + shared_out[...]).astype(jnp.bfloat16)
+                for e in range(experts):
+                    r_copy(k, e).wait_recv()
+
+            shared_out[...] = returned(k)
 
     routes_copy.wait_send()
     stream_copy.wait_send()
@@ -562,17 +595,20 @@
     up_copy.wait_send()
     down_copy.wait_send()
     finish_sends(mixed_block, 0, MIXED)
+    finish_sends(edges_block, 0, EDGES)
     finish_sends(sums_block, 0, SUMS)
     finish_sends(gains_block, 0, GAINS)
     finish_sends(whole_block, 0, WHOLE)
     finish_sends(shared_block, 0, SHARED)
 
-    finish_sends(hidden_block, 0, HIDDEN)
+    for e in range(experts):
+        finish_sends(hidden_block(e), 0, HIDDEN + e)
 
     @pl.loop(1, n_sp)
     def _(k):
-        finish_sends(hidden_block, k, HIDDEN + k)
-        r_copy(k).wait_send()
+        for e in range(experts):
+            finish_sends(hidden_block(e), k, HIDDEN + k * experts + e)
+            r_copy(k, e).wait_send()
 
         @pl.when(k != half)
         def _():
@@ -589,6 +625,10 @@
             for j in range(1, rows_y):
                 f_copy(block, k, DISPATCH + k, j).wait_send()
                 b_copy(k, j).wait_send()
+
+    for e in range(experts):
+        r_copy(combine[-1], e).wait_recv()
+    out[...] = (stream[...].astype(f32) + returned(combine[-1])).astype(jnp.bfloat16)
 
 
 def local(
@@ -614,7 +654,7 @@
     width = residual.shape[1]
     cap = 2 * token_count * routes.shape[1] // (experts * n_sp)
     cap = (cap + 15) // 16 * 16
-    slots = 2 * n_sp + 5
+    slots = n_sp * (1 + experts) + 6
     edge = min(128, token_count)
     lanes = (experts * cap + 127) // 128 * 128
     vmem = pl.BlockSpec(memory_space=pltpu.VMEM)
@@ -637,6 +677,8 @@
             pltpu.VMEM((channels, token_count), bf16),
             pltpu.VMEM((channels, edge), bf16),
             pltpu.VMEM((channels, edge), bf16),
+            pltpu.VMEM((channels * n_tp, token_count), bf16),
+            pltpu.VMEM((n_tp, channels, edge), bf16),
             pltpu.VMEM((channels * n_tp, token_count), bf16),
             pltpu.VMEM((n_tp, 8, token_count), jnp.float32),
             pltpu.VMEM((n_tp, 8, width), jnp.float32),
@@ -685,8 +727,8 @@
             dma((slots,)),
             dma((slots,)),
             dma((slots,)),
-            dma((n_sp,)),
-            dma((n_sp,)),
+            dma((n_sp, experts)),
+            dma((n_sp, experts)),
         ],
         compiler_params=pltpu.CompilerParams(
             collective_id=0, has_side_effects=True, vmem_limit_bytes=VMEM_LIMIT

time: 97.8 us -> 96 us (0.982)
  Pallas kernels: 96.9 us -> 95.1 us
    pallas_call x1, Pallas kernels: 96.9 us -> 95.1 us  [local(): pl.pallas_call(functools.partial(moe_kernel, n_sp, n_tp), name='moe', out...]
where the time goes in v3:
time: 96 us; the launch traced here: 95.8 us
  Pallas kernels  95.1 us (99%)
    pallas_call x1, Pallas kernels, local(): pl.pallas_call(functools.partial(moe_kernel, n_sp, n_tp), name='moe', out...  95.1 us

profile of v3, /device:TPU:0, one launch (start us, length us, event | category | flops | bytes accessed | tf_op | source)
XLA Modules:
  0.0 95.8 jit_solution(4524418288786032451)
XLA Ops:
  0.0 95.1 %moe.1 = bf16[384,512]{1,0:T(8,128)(2,1)S(1)} custom-call(bf16[128,384]{1,0:T(8,128)(2,1)} %outer_hbm.1, bf16[128,384]{1,0:T(8,128)(2,1)} %inner_hbm.1, bf16[128,384]{1,0:T(8,128)(2,1)} %conv_hbm.1, bf16[3,128]{1,0:T(4,128)(2,1)} %taps_hbm.1, bf16[512]{0:T(512)(128)(2,1)} %gain_hbm.1, s32[2,384]{1,0:T(2,128)} %bitcast.2, f32[2,384]{1,0:T(2,128)} %bitcast.3, ...), custom_call_target="tpu_custom_call" | custom-call | tf_op jit(solution)/shard_map/moe/pallas_call | solution.py:664
  95.1 0.7 copy.17

commit v4 on v3

--- a/solution.py
+++ b/solution.py
@@ -79,7 +79,6 @@
     sup,
     sdown,
     load_sem,
-    own_sem,
     h_send,
     h_recv,
     a_send,
@@ -382,11 +381,9 @@
             outgoing[k, e] = packed[e * cap : (e + 1) * cap]
         a_copy(k).start()
 
+    whole[:, pl.ds(pl.multiple_of(t * width, width), width)] = stream[...]
+    spread(whole_block, 0, WHOLE)
     stream_copy.start()
-    own_whole = pltpu.make_async_copy(stream, whole_block(0, t), own_sem)
-    own_whole.start()
-    own_whole.wait()
-    spread(whole_block, 0, WHOLE)
 
     @pl.loop(1, half)
     def _(k):
@@ -497,10 +494,6 @@
     for e in range(experts):
         recv[e, rows_of(half), pl.ds(pl.multiple_of(t * width, width), width)] = far_rows[e * cap : (e + 1) * cap]
     spread(block, half, DISPATCH + half)
-    @pl.loop(2, near)
-    def _(k):
-        pack_extra(k)
-
     normed[...] = (whole[...].astype(f32) * inverse_rms * gain_row[0:1]).astype(jnp.bfloat16)
     tokens = normed[...]
     shared_hidden = jax.nn.silu(jnp.dot(tokens, sgate[...], preferred_element_type=jnp.float32)) * jnp.dot(
@@ -517,6 +510,10 @@
     def _(k):
         inverse_out[k] = inverses(mate(k - half), far_column, far_rms)
         i_copy(k).start()
+
+    @pl.loop(2, near)
+    def _(k):
+        pack_extra(k)
 
     weight_rows = scores[...] / jnp.sum(scores[...], axis=0, keepdims=True) * routed_scale
     weights = [column_of(weight_rows[k : k + 1]) for k in range(choices)]
@@ -710,7 +707,6 @@
             pltpu.VMEM(shared_up.shape, bf16),
             pltpu.VMEM(shared_down.shape, bf16),
             dma((15,)),
-            dma,
             dma((2,)),
             dma((2,)),
             dma((n_sp,)),

time: 96 us -> 96 us (level)
  no operation moved by 1% of the time
where the time goes in v4:
time: 96 us; the launch traced here: 95.8 us
  Pallas kernels  95.1 us (99%)
    pallas_call x1, Pallas kernels, local(): pl.pallas_call(functools.partial(moe_kernel, n_sp, n_tp), name='moe', out...  95.1 us

profile of v4, /device:TPU:0, one launch (start us, length us, event | category | flops | bytes accessed | tf_op | source)
XLA Modules:
  0.0 95.8 jit_solution(11174736757154659881)
XLA Ops:
  0.0 95.1 %moe.1 = bf16[384,512]{1,0:T(8,128)(2,1)S(1)} custom-call(bf16[128,384]{1,0:T(8,128)(2,1)} %outer_hbm.1, bf16[128,384]{1,0:T(8,128)(2,1)} %inner_hbm.1, bf16[128,384]{1,0:T(8,128)(2,1)} %conv_hbm.1, bf16[3,128]{1,0:T(4,128)(2,1)} %taps_hbm.1, bf16[512]{0:T(512)(128)(2,1)} %gain_hbm.1, s32[2,384]{1,0:T(2,128)} %bitcast.2, f32[2,384]{1,0:T(2,128)} %bitcast.3, ...), custom_call_target="tpu_custom_call" | custom-call | tf_op jit(solution)/shard_map/moe/pallas_call | solution.py:661
  95.1 0.7 copy.17
